TPU v7x, 32 devices: a whole 2x2x4 slice. The times are simulated.
32 devices in a mesh: sp: 4 (over y, x), tp: 8 (over z, core).
Axes of the slice: x: 2, y: 2, z: 4, core: 2. Of those that a mesh axis runs over, the one named last changes fastest.
Arguments:
- queries: bfloat16 [2048, 1536], P('sp', 'tp'), may hold values from -34 to 34
- latent: bfloat16 [2048, 512], P('sp'), may hold values from -6 to 6
- rot_key: bfloat16 [2048, 32], P('sp'), may hold values from -34 to 34
- latent_gain: float32 [512], replicated, may hold values from 0.1 to 1.9
- key_up: bfloat16 [512, 1024], P(None, 'tp'), may hold values from -0.25 to 0.25
- value_up: bfloat16 [512, 1024], P(None, 'tp'), may hold values from -0.70710678 to 0.70710678
- query_gain: float32 [96], replicated, may hold values from 0.5 to 6
- key_gain: float32 [96], replicated, may hold values from 0.5 to 6
- out_gain: float32 [1024], replicated, may hold values from 0.1 to 1.9
- out_weight: bfloat16 [1024, 2048], replicated, may hold values from -0.1875 to 0.1875
- residual: bfloat16 [2048, 2048], P(('sp', 'tp')), may hold values from -6 to 6
- ffn_gain: float32 [2048], replicated, may hold values from 0.1 to 1.9
- routes: int32 [2048, 2], P(('sp', 'tp')), may hold values from 0 to 3, all different within a row; in each aligned block of 64 rows (0 to 63, 64 to 127, ...) at most 36 rows name the same one
- route_weights: float32 [2048, 2], P(('sp', 'tp')), may hold values from 0.2 to 1
- expert_gate: bfloat16 [4, 2048, 2048], P('sp', None, 'tp'), may hold values from -0.125 to 0.125
- expert_up: bfloat16 [4, 2048, 2048], P('sp', None, 'tp'), may hold values from -0.125 to 0.125
- expert_down: bfloat16 [4, 2048, 2048], P('sp', 'tp'), may hold values from -0.125 to 0.125
Outputs:
- layer_out: bfloat16 [2048, 2048], P(('sp', 'tp'))
Inputs may be any that keep to these rules, and one draw needn't show every extreme that they name: `routes`: the 2 experts of a token differ. Among the 64 rows of one device each expert is named by at most 36 rows, a bound that some block reaches.
All inputs are finite; a program needn't handle non-finite values.
Results may differ from a plain program's by a relative error of at most 0.02.
The roundings to bfloat16 on the way count: a program that leaves them out, or rounds other values in their place, can miss the bound.
Values may be sent and summed in bfloat16 or wider, within the bound.
No kernel may reach another device: no remote copies, remote signals or barrier semaphores. Data moves between devices by JAX's collectives and lax.ppermute only.
A program may use at most 128 MiB of HBM per device.

v0:
```python
import jax
import jax.numpy as jnp
from jax import lax
from jax.sharding import PartitionSpec as P

D = 2048
NOPE = 64
ROPE = 32
VH = 64
TOPK = 2
QK = 96
epsilon = 1e-06
rope_base = 10000.0


def rms_scale(values):
    return lax.rsqrt(jnp.mean(values * values, axis=-1, keepdims=True) + epsilon)


def rotate_half(values, angles):
    half_dims = values.shape[-1] // 2
    first_half = values[..., :half_dims]
    second_half = values[..., half_dims:]
    cosine = jnp.cos(angles)
    sine_val = jnp.sin(angles)
    return jnp.concatenate(
        [
            first_half * cosine - second_half * sine_val,
            second_half * cosine + first_half * sine_val,
        ],
        axis=-1,
    )


def head_prepare(raw_rows, gain_vec, angles):
    normed_rows = raw_rows * rms_scale(raw_rows) * gain_vec
    turned_rows = rotate_half(normed_rows[..., NOPE:], angles[:, None, :])
    return jnp.concatenate([normed_rows[..., :NOPE], turned_rows], axis=-1).astype(jnp.bfloat16)


def slot_targets(route_rows, expert_total, slot_cap):
    flat_routes = route_rows.reshape(-1)
    one_hot = (flat_routes[:, None] == jnp.arange(expert_total, dtype=jnp.int32)[None, :]).astype(
        jnp.int32
    )
    earlier = jnp.cumsum(one_hot, axis=0) - one_hot
    rank_in = jnp.sum(earlier * one_hot, axis=1)
    return (flat_routes * slot_cap + rank_in).reshape(route_rows.shape)


def select_matrix(targets, slot_total):
    hits = targets[:, :, None] == jnp.arange(slot_total, dtype=jnp.int32)[None, None, :]
    return jnp.sum(hits.astype(jnp.bfloat16), axis=1)


def shards(
    queries,
    latent,
    rot_key,
    latent_gain,
    key_up,
    value_up,
    query_gain,
    key_gain,
    out_gain,
    out_weight,
    residual,
    ffn_gain,
    routes,
    route_weights,
    expert_gate,
    expert_up,
    expert_down,
):
    shard_len = queries.shape[0]
    local_heads = key_up.shape[1] // NOPE
    sp_count = lax.axis_size("sp")
    tp_count = lax.axis_size("tp")
    my_first = lax.axis_index("sp") * shard_len
    my_last = my_first + shard_len - 1
    positions = my_first + jnp.arange(shard_len, dtype=jnp.int32)
    inverse = rope_base ** (-jnp.arange(0, ROPE, 2, dtype=jnp.float32) / ROPE)
    angles = positions.astype(jnp.float32)[:, None] * inverse[None, :]
    lat_f32 = latent.astype(jnp.float32)
    normed_latent = (lat_f32 * rms_scale(lat_f32) * latent_gain).astype(jnp.bfloat16)
    key_nope = jnp.dot(normed_latent, key_up, preferred_element_type=jnp.float32).astype(
        jnp.bfloat16
    )
    value_rows = jnp.dot(normed_latent, value_up, preferred_element_type=jnp.float32).astype(
        jnp.bfloat16
    )
    shared = jnp.broadcast_to(
        rot_key.astype(jnp.float32)[:, None, :], (shard_len, local_heads, ROPE)
    )
    raw_keys = jnp.concatenate(
        [key_nope.astype(jnp.float32).reshape(shard_len, local_heads, NOPE), shared], axis=-1
    )
    key_rows = head_prepare(raw_keys, key_gain, angles)
    query_rows = head_prepare(
        queries.astype(jnp.float32).reshape(shard_len, local_heads, QK), query_gain, angles
    )
    query_heads = jnp.transpose(query_rows, (1, 0, 2))
    bundle = jnp.concatenate(
        [
            jnp.transpose(key_rows, (1, 2, 0)),
            jnp.transpose(value_rows.reshape(shard_len, local_heads, VH), (1, 2, 0)),
        ],
        axis=1,
    )
    score_scale = QK ** (-0.5)
    init_state = (
        jnp.full((local_heads, shard_len), -1e30, jnp.float32),
        jnp.zeros((local_heads, shard_len), jnp.float32),
        jnp.zeros((local_heads, shard_len, VH), jnp.float32),
    )
    key_piece = lax.all_gather(bundle, "sp", axis=2, tiled=True)
    block_count = key_piece.shape[2] // shard_len

    def one_block(block_index, running_state):
        first_key = block_index * shard_len

        def compute(inner):
            row_peak, row_total, weighted = inner
            key_part = lax.dynamic_slice_in_dim(key_piece, block_index * shard_len, shard_len, 2)
            scores = (
                jnp.einsum(
                    "hqc,hck->hqk",
                    query_heads,
                    key_part[:, :QK, :],
                    preferred_element_type=jnp.float32,
                )
                * score_scale
            )
            key_pos = first_key + jnp.arange(shard_len, dtype=jnp.int32)
            allowed = key_pos[None, None, :] <= positions[None, :, None]
            scores = jnp.where(allowed, scores, -1e30)
            new_peak = jnp.maximum(row_peak, jnp.max(scores, axis=2))
            exponent = jnp.where(allowed, jnp.exp(scores - new_peak[..., None]), 0.0)
            factor = jnp.exp(row_peak - new_peak)
            new_total = row_total * factor + jnp.sum(exponent, axis=2)
            contrib = jnp.einsum(
                "hqk,hvk->hqv",
                exponent.astype(jnp.bfloat16),
                key_part[:, QK:, :],
                preferred_element_type=jnp.float32,
            )
            return (new_peak, new_total, weighted * factor[..., None] + contrib)

        return lax.cond(first_key <= my_last, compute, lambda inner: inner, running_state)

    row_peak, row_total, weighted = lax.fori_loop(0, block_count, one_block, init_state)
    attended = (weighted / row_total[..., None]).astype(jnp.bfloat16)
    tok_count = residual.shape[0]
    head_major = jnp.transpose(attended, (1, 0, 2)).reshape(shard_len, local_heads * VH)
    token_rows = lax.all_to_all(head_major, "tp", split_axis=0, concat_axis=1, tiled=True).astype(
        jnp.float32
    )
    normed_rows = (token_rows * rms_scale(token_rows) * out_gain).astype(jnp.bfloat16)
    partials = jnp.einsum(
        "tgc,gcd->tgd",
        normed_rows.reshape(tok_count, tp_count, -1),
        out_weight.reshape(tp_count, -1, D),
        preferred_element_type=jnp.float32,
    )
    rounded = lax.optimization_barrier(partials.astype(jnp.bfloat16))
    mixed = jnp.sum(rounded.astype(jnp.float32), axis=1)
    middle = residual.astype(jnp.float32) + mixed
    ffn_input = (middle * rms_scale(middle) * ffn_gain).astype(jnp.bfloat16)
    slot_cap = max(2, 9 * tok_count * TOPK // (8 * sp_count))
    slot_total = sp_count * slot_cap
    targets = slot_targets(routes, sp_count, slot_cap)
    chooser = select_matrix(targets, slot_total)
    outbound = (
        jnp.einsum("ts,td->sd", chooser, ffn_input, preferred_element_type=jnp.float32)
        .astype(jnp.bfloat16)
        .reshape(sp_count, slot_cap, D)
    )
    arrived = lax.all_to_all(outbound, "sp", split_axis=0, concat_axis=0, tiled=True)
    item_count = arrived.shape[1]
    flat_rows = arrived.reshape(sp_count * item_count, D)
    row_block = lax.all_gather(flat_rows, "tp", axis=0, tiled=True)
    gate_pre = jnp.dot(row_block, expert_gate[0], preferred_element_type=jnp.float32)
    up_pre = jnp.dot(row_block, expert_up[0], preferred_element_type=jnp.float32)
    hidden = (jax.nn.silu(gate_pre) * up_pre).astype(jnp.bfloat16)
    served = lax.psum_scatter(
        jnp.dot(hidden, expert_down[0], preferred_element_type=jnp.float32).astype(jnp.bfloat16),
        "tp",
        scatter_dimension=0,
        tiled=True,
    ).reshape(sp_count, item_count, D)
    returned_rows = lax.all_to_all(served, "sp", split_axis=0, concat_axis=0, tiled=True).reshape(
        slot_total, D
    )
    picked = (
        jnp.take(returned_rows, targets.reshape(-1), axis=0)
        .reshape(tok_count, TOPK, D)
        .astype(jnp.float32)
    )
    moe_sum = jnp.sum(picked * route_weights[:, :, None], axis=1)
    return (middle + moe_sum).astype(jnp.bfloat16)


def solution(mesh):
    return jax.shard_map(
        shards,
        mesh=mesh,
        in_specs=(
            P("sp", "tp"),
            P("sp", None),
            P("sp", None),
            P(),
            P(None, "tp"),
            P(None, "tp"),
            P(),
            P(),
            P(),
            P(),
            P(("sp", "tp"), None),
            P(),
            P(("sp", "tp"), None),
            P(("sp", "tp"), None),
            P("sp", None, "tp"),
            P("sp", None, "tp"),
            P("sp", "tp", None),
        ),
        out_specs=P(("sp", "tp"), None),
        check_vma=False,
    )
```

profile of v0, /device:TPU:0, one launch (start us, length us, event | category | flops | bytes accessed | tf_op | source)
XLA Modules:
  0.0 237.7 jit_solution(2543511276037347893)
XLA Ops:
  6.6 0.0 all-gather.3.cloned.1.call-start
  6.6 1.3 fusion.25
  8.0 1.5 bitcast_convert_fusion
  9.5 0.8 broadcast_in_dim.40
  10.3 0.1 fusion.34
  10.5 0.0 copy-start.4
  10.5 0.1 fusion.35
  10.6 0.4 convolution_convert_fusion.3
  11.1 0.2 multiply_cosine_fusion
  11.3 0.8 pad_maximum_fusion.1
  12.1 0.0 all-gather.3.cloned.1.call-update
  12.2 0.1 copy.47
  12.3 0.1 reshape.250
  12.4 0.1 fusion.50
  12.5 0.2 reduce_window_sum.11
  12.7 0.2 select_reduce_fusion
  12.9 0.1 reduce_sum.103
  13.0 0.1 copy.48
  13.1 0.7 maximum_bitcast_fusion.1
  13.8 29.8 %all-gather.3.cloned.1.call-done = bf16[2,160,2048]{2,1,0:T(8,128)(2,1)} async-done(((bf16[2,160,512]{2,1,0:T(8,128)(2,1)}), bf16[2,160,2048]{2,1,0:T(8,128)(2,1)}) %all-gather.3.cloned.1.call-update) | async-done | bytes 1310736 | tf_op jit(solution)/shard_map/all_gather | solution.py:116
  43.6 0.7 broadcast_in_dim.39
  44.3 5.1 %while.18 = (s32[]{:T(128)}, f32[2,512]{1,0:T(2,128)S(1)}, f32[2,512]{1,0:T(2,128)S(1)}, f32[2,512,64]{1,2,0:T(8,128)}, s32[]{:T(128)}, /*index=5*/bf16[2,160,20...) while((s32[]{:T(128)}, f32[2,512]{1,0:T(2,128)S(1)}, ...), condition=%wide.region_8.9_spmd.clone, body=%wide.region_3.8_spmd.clone.sunk | while | flops 174984192 | bytes 8466765 | solution.py:151
  44.3 5.0 %conditional.3 = ((f32[2,512]{1,0:T(2,128)S(1)}, f32[2,512]{1,0:T(2,128)S(1)}, f32[2,512,64]{1,2,0:T(8,128)})) conditional(s32[]{:T(128)} %convert_element_type.181, (f32[2,512]{1,0:T(2,128)S(1)}, f32[2,512]{1,0:T(2,128)S(1)}, f32[2,512,64]{1,2,0:T(8,128)}) %tuple.52, (s32[]{:T(128)}, s32[]{:T(128)}, s32[]{:T(128)}, bf16[2,160,2048]{2,1,0:T(8,128)(2,1)}, ...), branch_computations={%region_4.0_spmd, %region_5.7_spmd} | conditional | flops 174984192 | bytes 8464494 | solution.py:149
  44.3 0.2 broadcast_compare_fusion
  44.6 1.7 fusion.2
  46.3 0.6 fusion.4
  46.8 2.5 %convolution_add_fusion = f32[2,512,64]{1,2,0:T(8,128)} fusion(f32[2,512,512]{2,1,0:T(8,128)S(1)} %get-tuple-element.232, f32[2,512]{1,0:T(2,128)S(1)} %max.2, pred[512,512]{0,1:T(8,128)(4,1)S(1)} %broadcast_compare_fusion, f32[2,512,64]{1,2,0:T(8,128)} %get-tuple-element.169, bf16[2,160,2048]{2,1,0:T(8,128)(2,1)} %get-tuple-element.165, s32[]{:T(128)S(6)} %add.179, ...), kind=kOutput, calls=%fused_computation.7 | convolution fusion | flops 69861376 | bytes 3022856 | tf_op jit(solution)/shard_map/while/body/eval_jaxpr/cond/branch_1_fun/hqk,hvk->hqv/dot_general | solution.py:141
  49.4 1.0 fusion.47
  50.4 0.2 all_to_all.16
  50.6 0.8 copy.46
  51.5 4.6 %all-to-all-start = ((bf16[8,64,128]{2,1,0:T(8,128)(2,1)}), bf16[8,64,128]{2,1,0:T(8,128)(2,1)S(1)}, u32[]{:S(2)}, u32[]{:S(2)}) async-start(bf16[8,64,128]{2,1,0:T(8,128)(2,1)} %copy.46), calls=%async_computation | async-start | bytes 262144 | tf_op jit(solution)/shard_map/all_to_all | solution.py:155
  56.1 0.0 all-gather.5.cloned.1.call-start
  56.1 0.1 fusion.49
  56.2 6.6 %all-to-all-done = bf16[8,64,128]{2,1,0:T(8,128)(2,1)S(1)} async-done(((bf16[8,64,128]{2,1,0:T(8,128)(2,1)}), bf16[8,64,128]{2,1,0:T(8,128)(2,1)S(1)}, u32[]{:S(2)}, u32[]{:S(2)}) %all-to-all-start) | async-done | bytes 131104 | tf_op jit(solution)/shard_map/all_to_all | solution.py:155
  62.8 0.1 fusion.36
  62.9 3.0 %fusion.18 = bf16[64,8,2048]{2,0,1:T(8,128)(2,1)S(1)} fusion(bf16[8,128,2048]{2,1,0:T(8,128)(2,1)} %bitcast.57, bf16[8,64,128]{2,1,0:T(8,128)(2,1)S(1)} %all-to-all-done, f32[8,128]{1,0:T(8,128)S(1)} %bitcast.61, f32[64]{0:T(128)S(1)} %add_rsqrt_fusion.4), kind=kOutput, calls=%fused_computation.29 | convolution fusion | flops 269746176 | bytes 6426880 | tf_op jit(solution)/shard_map/tgc,gcd->tgd/dot_general | solution.py:159
  65.9 0.0 copy-start.1
  65.9 0.4 convert_reduce_fusion
  66.3 0.6 copy-done.1
  66.9 0.2 multiply_reduce_fusion.1
  67.1 0.4 convolution_convert_fusion.2
  67.4 0.1 reshape.251
  67.6 27.1 %all_to_all.23 = bf16[4,36,2048]{2,1,0:T(8,128)(2,1)S(1)} all-to-all(bf16[4,36,2048]{2,1,0:T(8,128)(2,1)S(1)} %reshape.251), channel_id=1, replica_groups=mesh['sp'=4,'tp'=8] {'sp'}, dimensions={0} | all-to-all | bytes 1179648 | tf_op jit(solution)/shard_map/all_to_all | solution.py:178
  94.7 1.0 reshape.252
  95.6 0.0 all-gather.5.cloned.1.call-update
  95.7 0.2 reduce-scatter.2.cloned.1.call-start
  95.9 48.8 %all-gather.5.cloned.1.call-done = bf16[1152,2048]{1,0:T(8,128)(2,1)} async-done(((bf16[144,2048]{1,0:T(8,128)(2,1)}), bf16[1152,2048]{1,0:T(8,128)(2,1)}) %all-gather.5.cloned.1.call-update) | async-done | bytes 4718608 | tf_op jit(solution)/shard_map/all_gather | solution.py:181
  144.7 5.0 %fusion.31 = f32[1152,256]{1,0:T(8,128)} fusion(bf16[1152,2048]{1,0:T(8,128)(2,1)} %all-gather.5.cloned.1.call-done, bf16[1,2048,256]{2,1,0:T(8,128)(2,1)} %param.35), kind=kOutput, calls=%fused_computation.46 | convolution fusion | flops 1207959552 | bytes 6946816 | tf_op jit(solution)/shard_map/dot_general | solution.py:182
  149.7 9.7 %convolution_convert_fusion = bf16[1152,2048]{1,0:T(8,128)(2,1)} fusion(bf16[1152,2048]{1,0:T(8,128)(2,1)} %all-gather.5.cloned.1.call-done, f32[1152,256]{1,0:T(8,128)} %fusion.31, bf16[1,256,2048]{2,1,0:T(8,128)(2,1)S(1)} %copy-done, bf16[1,2048,256]{2,1,0:T(8,128)(2,1)S(1)} %copy-done.10), kind=kOutput, calls=%fused_computation.25 | convolution fusion | flops 2420047872 | bytes 12713984 | tf_op jit(solution)/shard_map/dot_general | solution.py:186
  159.4 0.0 reduce-scatter.2.cloned.1.call-update
  159.5 0.0 copy-start.7
  159.5 53.8 %reduce-scatter.2.cloned.1.call-done = bf16[144,2048]{1,0:T(8,128)(2,1)} async-done(((bf16[1152,2048]{1,0:T(8,128)(2,1)}), bf16[144,2048]{1,0:T(8,128)(2,1)}) %reduce-scatter.2.cloned.1.call-update) | async-done | bytes 589840 | tf_op jit(solution)/shard_map/reduce_scatter | solution.py:185
  213.3 2.0 reshape.253
  215.3 3.6 %all-to-all-start.2 = ((bf16[4,36,2048]{2,1,0:T(8,128)(2,1)}), bf16[4,36,2048]{2,1,0:T(8,128)(2,1)S(1)}, u32[]{:S(2)}, u32[]{:S(2)}) async-start(bf16[4,36,2048]{2,1,0:T(8,128)(2,1)} %reshape.253), calls=%async_computation.3 | async-start | bytes 1310720 | tf_op jit(solution)/shard_map/all_to_all | solution.py:191
  218.9 0.1 copy.50
  219.0 0.1 mul.297
  219.2 0.1 copy.49
  219.3 0.1 copy.51
  219.4 7.2 %all-to-all-done.2 = bf16[4,36,2048]{2,1,0:T(8,128)(2,1)S(1)} async-done(((bf16[4,36,2048]{2,1,0:T(8,128)(2,1)}), bf16[4,36,2048]{2,1,0:T(8,128)(2,1)S(1)}, u32[]{:S(2)}, u32[]{:S(2)}) %all-to-all-start.2) | async-done | bytes 589856 | tf_op jit(solution)/shard_map/all_to_all | solution.py:191
  226.6 0.1 reshape.254
  226.7 0.9 gather_fusion
  227.7 0.3 gather.7
  228.0 2.3 multiply_reduce_fusion
  230.4 0.8 add_convert_fusion
  (51 shorter events, 0.3 us)
Async XLA Ops:
  6.5 143.2 %copy-start = (bf16[1,256,2048]{2,1,0:T(8,128)(2,1)S(1)}, bf16[1,256,2048]{2,1,0:T(8,128)(2,1)}, u32[]{:S(2)}) copy-start(bf16[1,256,2048]{2,1,0:T(8,128)(2,1)} %param.37) | copy-start | bytes 3145732
  6.5 4.1 %copy-start.3 = (bf16[512,512]{1,0:T(8,128)(2,1)S(1)}, bf16[512,512]{1,0:T(8,128)(2,1)}, u32[]{:S(2)}) copy-start(bf16[512,512]{1,0:T(8,128)(2,1)} %param.22) | copy-start | bytes 1572868
  6.5 4.1 %copy-start.12 = (f32[512]{0:T(512)S(1)}, f32[512]{0:T(512)}, u32[]{:S(2)}) copy-start(f32[512]{0:T(512)} %param.24) | copy-start | bytes 6148
  6.5 3.8 %copy-start.2 = (bf16[512,192]{0,1:T(8,128)(2,1)S(1)}, bf16[512,192]{0,1:T(8,128)(2,1)}, u32[]{:S(2)}) copy-start(bf16[512,192]{0,1:T(8,128)(2,1)} %param.21) | copy-start | bytes 589828
  6.5 3.9 %copy-start.8 = (f32[96]{0:T(128)S(1)}, f32[96]{0:T(128)}, u32[]{:S(2)}) copy-start(f32[96]{0:T(128)} %param.27) | copy-start | bytes 1156
  6.5 3.9 %copy-start.9 = (f32[96]{0:T(128)S(1)}, f32[96]{0:T(128)}, u32[]{:S(2)}) copy-start(f32[96]{0:T(128)} %param.28) | copy-start | bytes 1156
  6.6 4.1 %copy-start.11 = (bf16[512,128]{1,0:T(8,128)(2,1)S(1)}, bf16[512,128]{1,0:T(8,128)(2,1)}, u32[]{:S(2)}) copy-start(bf16[512,128]{1,0:T(8,128)(2,1)} %param.26) | copy-start | bytes 393220
  6.6 37.0 %all-gather.3.cloned.1.call-start = ((), (), s32[]{:S(2)}) async-start(), calls=%async_computation.4 | async-start | bytes 1638400 | tf_op jit(solution)/shard_map/all_gather | solution.py:116
  10.5 1.7 copy-start.4
  44.3 18.6 %copy-start.6 = (f32[1024]{0:T(1024)S(1)}, f32[1024]{0:T(1024)}, u32[]{:S(2)}) copy-start(f32[1024]{0:T(1024)} %param.29) | copy-start | bytes 12292
  51.5 11.3 %all-to-all-start = ((bf16[8,64,128]{2,1,0:T(8,128)(2,1)}), bf16[8,64,128]{2,1,0:T(8,128)(2,1)S(1)}, u32[]{:S(2)}, u32[]{:S(2)}) async-start(bf16[8,64,128]{2,1,0:T(8,128)(2,1)} %copy.46), calls=%async_computation | async-start | bytes 262144 | tf_op jit(solution)/shard_map/all_to_all | solution.py:155
  56.1 88.6 %all-gather.5.cloned.1.call-start = ((), (), s32[]{:S(2)}) async-start(), calls=%async_computation.5 | async-start | bytes 5308416 | tf_op jit(solution)/shard_map/all_gather | solution.py:181
  65.9 1.0 copy-start.1
  65.9 1.1 copy-start.5
  95.6 54.1 %copy-start.10 = (bf16[1,2048,256]{2,1,0:T(8,128)(2,1)S(1)}, bf16[1,2048,256]{2,1,0:T(8,128)(2,1)}, u32[]{:S(2)}) copy-start(bf16[1,2048,256]{2,1,0:T(8,128)(2,1)} %param.36) | copy-start | bytes 3145732
  95.7 117.6 %reduce-scatter.2.cloned.1.call-start = ((), (), s32[]{:S(2)}) async-start(), calls=%async_computation.6 | async-start | bytes 5308416 | tf_op jit(solution)/shard_map/reduce_scatter | solution.py:185
  159.5 59.8 %copy-start.7 = (f32[64,2]{0,1:T(2,128)S(1)}, f32[64,2]{0,1:T(2,128)}, u32[]{:S(2)}) copy-start(f32[64,2]{0,1:T(2,128)} %param.34) | copy-start | bytes 1540
  215.3 11.3 %all-to-all-start.2 = ((bf16[4,36,2048]{2,1,0:T(8,128)(2,1)}), bf16[4,36,2048]{2,1,0:T(8,128)(2,1)S(1)}, u32[]{:S(2)}, u32[]{:S(2)}) async-start(bf16[4,36,2048]{2,1,0:T(8,128)(2,1)} %reshape.253), calls=%async_computation.3 | async-start | bytes 1310720 | tf_op jit(solution)/shard_map/all_to_all | solution.py:191
Sparse Core Ops, SparseCore 0:
  12.3 31.2 all-gather.2
  95.8 48.8 all-gather.4
  159.6 53.6 reduce-scatter.1
where the time goes:
time: 238 us
  waiting for transfers between devices  146 us (61%)
  blocking collectives  27.1 us (11%)
  matrix products  24.2 us (10%)
  between operations  13.5 us (6%)
  other arithmetic  9.45 us (4%)
  local copies, waits for them, and re-layouts  8.58 us (4%)
  starting transfers between devices  8.54 us (4%)
    reduce_scatter x1, waiting for transfers between devices, shards(): lax.psum_scatter(jnp.dot(hidden, expert_down[0], preferred_element_type=j...  53.8 us
    all_gather x1, waiting for transfers between devices, shards(): row_block = lax.all_gather(flat_rows, 'tp', axis=0, tiled=True)  48.8 us
    all_gather x1, waiting for transfers between devices, shards(): key_piece = lax.all_gather(bundle, 'sp', axis=2, tiled=True)  29.8 us
    all_to_all x1, blocking collectives, shards(): lax.all_to_all(outbound, 'sp', split_axis=0, concat_axis=0, tiled=True)  27.1 us
    dot_general x1, matrix products, shards(): jnp.dot(hidden, expert_down[0], preferred_element_type=jnp.float32)  9.73 us
    all_to_all x1, waiting for transfers between devices, shards(): lax.all_to_all(served, 'sp', split_axis=0, concat_axis=0, tiled=True)  7.23 us
    all_to_all x1, waiting for transfers between devices, shards(): lax.all_to_all(head_major, 'tp', split_axis=0, concat_axis=1, tiled=True)  6.6 us
    dot_general x1, matrix products, shards(): jnp.dot(row_block, expert_gate[0], preferred_element_type=jnp.float32)  5.04 us
  transfers between devices with their start and end apart: 5, of which 5 were waited for; matrix products, arithmetic and copies ran while one was open for 1% of the time, Pallas kernels for 0%

commit v1 on v0

--- a/solution.py
+++ b/solution.py
@@ -72,6 +72,24 @@
     expert_up,
     expert_down,
 ):
+
+    def _trace_zone(named_axis, view):
+        n_now, then = (lax.psum(1, axis_name=named_axis), lax.axis_index(named_axis))
+        state_now = view.shape[0] // n_now
+        all_values = list(view.shape)
+        all_values[0] = state_now
+        y1 = all_values[1]
+        all_values[1] = y1 * n_now
+        mixed_arr = jnp.zeros(all_values, view.dtype)
+        for no in [*range(n_now)]:
+            b_now = lax.dynamic_slice_in_dim(view, (then ^ no) * state_now, state_now, axis=0)
+            if no:
+                b_now = lax.ppermute(
+                    b_now, axis_name=named_axis, perm=[(i0, i0 ^ no) for i0 in range(n_now)]
+                )
+            mixed_arr = lax.dynamic_update_slice_in_dim(mixed_arr, b_now, (then ^ no) * y1, axis=1)
+        return mixed_arr
+
     shard_len = queries.shape[0]
     local_heads = key_up.shape[1] // NOPE
     sp_count = lax.axis_size("sp")
@@ -152,9 +170,7 @@
     attended = (weighted / row_total[..., None]).astype(jnp.bfloat16)
     tok_count = residual.shape[0]
     head_major = jnp.transpose(attended, (1, 0, 2)).reshape(shard_len, local_heads * VH)
-    token_rows = lax.all_to_all(head_major, "tp", split_axis=0, concat_axis=1, tiled=True).astype(
-        jnp.float32
-    )
+    token_rows = _trace_zone("tp", head_major).astype(jnp.float32)
     normed_rows = (token_rows * rms_scale(token_rows) * out_gain).astype(jnp.bfloat16)
     partials = jnp.einsum(
         "tgc,gcd->tgd",

time: 238 us -> 240 us (level)
  starting transfers between devices: 8.54 us -> 12.4 us
  waiting for transfers between devices: 146 us -> 143 us
    ppermute x0 -> x7, starting transfers between devices: none -> 8.5 us  [_trace_zone(): lax.ppermute(b_now, axis_name=named_axis, perm=[(i0, i0 ^ no) for i0 in r...]
    all_to_all x1 -> x0, waiting for transfers between devices: 6.6 us -> none  [shards(): lax.all_to_all(head_major, 'tp', split_axis=0, concat_axis=1, tiled=True)]
    all_to_all x1 -> x0, starting transfers between devices: 4.6 us -> none  [shards(): lax.all_to_all(head_major, 'tp', split_axis=0, concat_axis=1, tiled=True)]
    ppermute x0 -> x7, waiting for transfers between devices: none -> 4.56 us  [_trace_zone(): lax.ppermute(b_now, axis_name=named_axis, perm=[(i0, i0 ^ no) for i0 in r...]
  transfers between devices with their start and end apart: 5 -> 11, of which waited for: 5 -> 6; matrix products, arithmetic and copies ran while one was open for 1% -> 1% of each run, Pallas kernels for 0% -> 0%
where the time goes in v1:
time: 240 us; the launch traced here: 239 us
  waiting for transfers between devices  143 us (60%)
  blocking collectives  27.8 us (12%)
  matrix products  24.2 us (10%)
  between operations  13.7 us (6%)
  starting transfers between devices  12.4 us (5%)
  other arithmetic  9.44 us (4%)
  local copies, waits for them, and re-layouts  8.5 us (4%)
    reduce_scatter x1, waiting for transfers between devices, shards(): lax.psum_scatter(jnp.dot(hidden, expert_down[0], preferred_element_type=j...  53.8 us
    all_gather x1, waiting for transfers between devices, shards(): row_block = lax.all_gather(flat_rows, 'tp', axis=0, tiled=True)  47.8 us
    all_gather x1, waiting for transfers between devices, shards(): key_piece = lax.all_gather(bundle, 'sp', axis=2, tiled=True)  29.5 us
    all_to_all x1, blocking collectives, shards(): lax.all_to_all(outbound, 'sp', split_axis=0, concat_axis=0, tiled=True)  27.8 us
    dot_general x1, matrix products, shards(): jnp.dot(hidden, expert_down[0], preferred_element_type=jnp.float32)  9.72 us
    ppermute x7, starting transfers between devices, _trace_zone(): lax.ppermute(b_now, axis_name=named_axis, perm=[(i0, i0 ^ no) for i0 in r...  8.5 us
    all_to_all x1, waiting for transfers between devices, shards(): lax.all_to_all(served, 'sp', split_axis=0, concat_axis=0, tiled=True)  7.2 us
    dot_general x1, matrix products, shards(): jnp.dot(row_block, expert_gate[0], preferred_element_type=jnp.float32)  5.04 us
  transfers between devices with their start and end apart: 11, of which 6 were waited for; matrix products, arithmetic and copies ran while one was open for 1% of the time, Pallas kernels for 0%

profile of v1, /device:TPU:0, one launch (start us, length us, event | category | flops | bytes accessed | tf_op | source)
XLA Modules:
  0.0 239.1 jit_solution(7476746043038087122)
XLA Ops:
  6.6 1.3 fusion.25
  8.0 1.5 bitcast_convert_fusion
  9.5 0.8 broadcast_in_dim.43
  10.5 0.1 fusion.35
  10.6 0.4 convolution_convert_fusion.3
  11.1 0.2 multiply_cosine_fusion
  11.3 0.8 pad_maximum_fusion.1
  12.3 0.1 copy.59
  12.4 0.1 reshape.242
  12.5 0.1 fusion.48
  12.6 0.2 reduce_window_sum.11
  12.8 0.2 select_reduce_fusion
  13.0 0.1 reduce_sum.103
  13.2 0.1 fusion.47
  13.3 0.7 maximum_bitcast_fusion.1
  14.0 29.5 %all-gather.3.cloned.1.call-done = bf16[2,160,2048]{2,1,0:T(8,128)(2,1)} async-done(((bf16[2,160,512]{2,1,0:T(8,128)(2,1)}), bf16[2,160,2048]{2,1,0:T(8,128)(2,1)}) %all-gather.3.cloned.1.call-update) | async-done | bytes 1310736 | tf_op jit(solution)/shard_map/all_gather | solution.py:134
  43.6 0.7 broadcast_in_dim.42
  44.3 5.1 %while.18 = (s32[]{:T(128)}, f32[2,512]{1,0:T(2,128)S(1)}, f32[2,512]{1,0:T(2,128)S(1)}, f32[2,512,64]{1,2,0:T(8,128)}, s32[]{:T(128)}, /*index=5*/bf16[2,160,20...) while((s32[]{:T(128)}, f32[2,512]{1,0:T(2,128)S(1)}, ...), condition=%wide.region_8.9_spmd.clone, body=%wide.region_3.8_spmd.clone.sunk | while | flops 174984192 | bytes 8466765 | solution.py:169
  44.3 5.0 %conditional.3 = ((f32[2,512]{1,0:T(2,128)S(1)}, f32[2,512]{1,0:T(2,128)S(1)}, f32[2,512,64]{1,2,0:T(8,128)})) conditional(s32[]{:T(128)} %convert_element_type.173, (f32[2,512]{1,0:T(2,128)S(1)}, f32[2,512]{1,0:T(2,128)S(1)}, f32[2,512,64]{1,2,0:T(8,128)}) %tuple.59, (s32[]{:T(128)}, s32[]{:T(128)}, s32[]{:T(128)}, bf16[2,160,2048]{2,1,0:T(8,128)(2,1)}, ...), branch_computations={%region_4.0_spmd, %region_5.7_spmd} | conditional | flops 174984192 | bytes 8464494 | solution.py:167
  44.3 0.2 broadcast_compare_fusion
  44.6 1.7 fusion.2
  46.2 0.6 fusion.4
  46.8 2.5 %convolution_add_fusion = f32[2,512,64]{1,2,0:T(8,128)} fusion(f32[2,512,512]{2,1,0:T(8,128)S(1)} %get-tuple-element.232, f32[2,512]{1,0:T(2,128)S(1)} %max.2, pred[512,512]{0,1:T(8,128)(4,1)S(1)} %broadcast_compare_fusion, f32[2,512,64]{1,2,0:T(8,128)} %get-tuple-element.169, bf16[2,160,2048]{2,1,0:T(8,128)(2,1)} %get-tuple-element.165, s32[]{:T(128)S(6)} %add.243, ...), kind=kOutput, calls=%fused_computation.7 | convolution fusion | flops 69861376 | bytes 3022856 | tf_op jit(solution)/shard_map/while/body/eval_jaxpr/cond/branch_1_fun/hqk,hvk->hqv/dot_general | solution.py:159
  49.4 1.0 divide_convert_fusion
  50.4 0.2 constant_dynamic-slice_fusion
  50.6 0.1 copy.65
  50.7 0.1 copy.66
  50.9 0.1 copy.67
  51.0 1.5 collective-permute-start.1
  52.6 0.4 collective-permute-start.2
  53.1 2.5 %collective-permute-start.3 = (bf16[64,128]{1,0:T(8,128)(2,1)S(1)}, bf16[64,128]{1,0:T(8,128)(2,1)S(1)}, u32[]{:S(2)}, u32[]{:S(2)}) collective-permute-start(bf16[64,128]{1,0:T(8,128)(2,1)S(1)} %copy.69), channel_id=1, source_target_pairs={{0,4},{1,5},{2,6},{3,7},{4,0},{5,1},{6,2},{7,3},{8,12},{9,13},{10,... | collective-permute-start | bytes 49160 | tf_op jit(solution)/shard_map/ppermute | solution.py:87
  55.7 0.2 collective-permute-start.4
  55.9 0.1 copy.71
  56.0 0.1 copy.72
  56.1 3.4 %collective-permute-start.5 = (bf16[64,128]{1,0:T(8,128)(2,1)S(1)}, bf16[64,128]{1,0:T(8,128)(2,1)S(1)}, u32[]{:S(2)}, u32[]{:S(2)}) collective-permute-start(bf16[64,128]{1,0:T(8,128)(2,1)S(1)} %copy.71), channel_id=1, source_target_pairs={{0,6},{1,7},{2,4},{3,5},{4,2},{5,3},{6,0},{7,1},{8,14},{9,15},{10,... | collective-permute-start | bytes 49160 | tf_op jit(solution)/shard_map/ppermute | solution.py:87
  59.5 0.4 collective-permute-start.6
  60.0 1.7 collective-permute-done.5
  61.7 2.8 %collective-permute-done.6 = bf16[64,128]{1,0:T(8,128)(2,1)S(1)} collective-permute-done((bf16[64,128]{1,0:T(8,128)(2,1)S(1)}, bf16[64,128]{1,0:T(8,128)(2,1)S(1)}, u32[]{:S(2)}, u32[]{:S(2)}) %collective-permute-start.6) | collective-permute-done | bytes 16416 | tf_op jit(solution)/shard_map/ppermute | solution.py:87
  64.6 0.1 fusion.36
  64.7 3.0 %fusion.18 = bf16[64,8,2048]{2,0,1:T(8,128)(2,1)S(1)} fusion(bf16[8,128,2048]{2,1,0:T(8,128)(2,1)} %bitcast.59, bf16[64,1024]{1,0:T(8,128)(2,1)S(1)} %constant_dynamic-update-slice_fusion, f32[1024]{0:T(1024)S(1)} %copy-done.6, f32[64]{0:T(128)S(1)} %add_rsqrt_fusion.4), kind=kOutput, calls=%fused_computation.29 | convolution fusion | flops 269746176 | bytes 6426880 | tf_op jit(solution)/shard_map/tgc,gcd->tgd/dot_general | solution.py:175
  67.7 0.4 convert_reduce_fusion
  68.1 0.6 copy-done.1
  68.6 0.2 multiply_reduce_fusion.1
  68.8 0.4 convolution_convert_fusion.2
  69.2 0.1 reshape.243
  69.3 27.8 %all_to_all.10 = bf16[4,36,2048]{2,1,0:T(8,128)(2,1)S(1)} all-to-all(bf16[4,36,2048]{2,1,0:T(8,128)(2,1)S(1)} %reshape.243), channel_id=1, replica_groups=mesh['sp'=4,'tp'=8] {'sp'}, dimensions={0} | all-to-all | bytes 1179648 | tf_op jit(solution)/shard_map/all_to_all | solution.py:194
  97.1 0.9 reshape.244
  98.1 0.2 reduce-scatter.2.cloned.1.call-start
  98.3 47.8 %all-gather.5.cloned.1.call-done = bf16[1152,2048]{1,0:T(8,128)(2,1)} async-done(((bf16[144,2048]{1,0:T(8,128)(2,1)}), bf16[1152,2048]{1,0:T(8,128)(2,1)}) %all-gather.5.cloned.1.call-update) | async-done | bytes 4718608 | tf_op jit(solution)/shard_map/all_gather | solution.py:197
  146.1 5.0 %fusion.31 = f32[1152,256]{1,0:T(8,128)} fusion(bf16[1152,2048]{1,0:T(8,128)(2,1)} %all-gather.5.cloned.1.call-done, bf16[1,2048,256]{2,1,0:T(8,128)(2,1)} %param.35), kind=kOutput, calls=%fused_computation.46 | convolution fusion | flops 1207959552 | bytes 6946816 | tf_op jit(solution)/shard_map/dot_general | solution.py:198
  151.1 9.7 %convolution_convert_fusion = bf16[1152,2048]{1,0:T(8,128)(2,1)} fusion(bf16[1152,2048]{1,0:T(8,128)(2,1)} %all-gather.5.cloned.1.call-done, f32[1152,256]{1,0:T(8,128)} %fusion.31, bf16[1,256,2048]{2,1,0:T(8,128)(2,1)S(1)} %copy-done, bf16[1,2048,256]{2,1,0:T(8,128)(2,1)S(1)} %copy-done.10), kind=kOutput, calls=%fused_computation.25 | convolution fusion | flops 2420047872 | bytes 12713984 | tf_op jit(solution)/shard_map/dot_general | solution.py:202
  160.9 53.8 %reduce-scatter.2.cloned.1.call-done = bf16[144,2048]{1,0:T(8,128)(2,1)} async-done(((bf16[1152,2048]{1,0:T(8,128)(2,1)}), bf16[144,2048]{1,0:T(8,128)(2,1)}) %reduce-scatter.2.cloned.1.call-update) | async-done | bytes 589840 | tf_op jit(solution)/shard_map/reduce_scatter | solution.py:201
  214.7 2.0 reshape.245
  216.7 3.6 %all-to-all-start.1 = ((bf16[4,36,2048]{2,1,0:T(8,128)(2,1)}), bf16[4,36,2048]{2,1,0:T(8,128)(2,1)S(1)}, u32[]{:S(2)}, u32[]{:S(2)}) async-start(bf16[4,36,2048]{2,1,0:T(8,128)(2,1)} %reshape.245), calls=%async_computation.2 | async-start | bytes 1310720 | tf_op jit(solution)/shard_map/all_to_all | solution.py:207
  220.4 0.1 copy.62
  220.5 0.1 mul.352
  220.6 0.1 copy.61
  220.7 0.1 copy.63
  220.8 7.2 %all-to-all-done.1 = bf16[4,36,2048]{2,1,0:T(8,128)(2,1)S(1)} async-done(((bf16[4,36,2048]{2,1,0:T(8,128)(2,1)}), bf16[4,36,2048]{2,1,0:T(8,128)(2,1)S(1)}, u32[]{:S(2)}, u32[]{:S(2)}) %all-to-all-start.1) | async-done | bytes 589856 | tf_op jit(solution)/shard_map/all_to_all | solution.py:207
  228.0 0.1 reshape.246
  228.2 0.9 gather_fusion
  229.1 0.3 gather.7
  229.4 2.3 multiply_reduce_fusion
  231.8 0.8 add_convert_fusion
  (79 shorter events, 1.1 us)
Async XLA Ops:
  6.5 144.6 %copy-start = (bf16[1,256,2048]{2,1,0:T(8,128)(2,1)S(1)}, bf16[1,256,2048]{2,1,0:T(8,128)(2,1)}, u32[]{:S(2)}) copy-start(bf16[1,256,2048]{2,1,0:T(8,128)(2,1)} %param.37) | copy-start | bytes 3145732
  6.5 4.1 %copy-start.3 = (bf16[512,512]{1,0:T(8,128)(2,1)S(1)}, bf16[512,512]{1,0:T(8,128)(2,1)}, u32[]{:S(2)}) copy-start(bf16[512,512]{1,0:T(8,128)(2,1)} %param.22) | copy-start | bytes 1572868
  6.5 4.1 %copy-start.12 = (f32[512]{0:T(512)S(1)}, f32[512]{0:T(512)}, u32[]{:S(2)}) copy-start(f32[512]{0:T(512)} %param.24) | copy-start | bytes 6148
  6.5 3.8 %copy-start.2 = (bf16[512,192]{0,1:T(8,128)(2,1)S(1)}, bf16[512,192]{0,1:T(8,128)(2,1)}, u32[]{:S(2)}) copy-start(bf16[512,192]{0,1:T(8,128)(2,1)} %param.21) | copy-start | bytes 589828
  6.5 3.9 %copy-start.8 = (f32[96]{0:T(128)S(1)}, f32[96]{0:T(128)}, u32[]{:S(2)}) copy-start(f32[96]{0:T(128)} %param.27) | copy-start | bytes 1156
  6.5 3.9 %copy-start.9 = (f32[96]{0:T(128)S(1)}, f32[96]{0:T(128)}, u32[]{:S(2)}) copy-start(f32[96]{0:T(128)} %param.28) | copy-start | bytes 1156
  6.6 4.1 %copy-start.11 = (bf16[512,128]{1,0:T(8,128)(2,1)S(1)}, bf16[512,128]{1,0:T(8,128)(2,1)}, u32[]{:S(2)}) copy-start(bf16[512,128]{1,0:T(8,128)(2,1)} %param.26) | copy-start | bytes 393220
  6.6 37.0 %all-gather.3.cloned.1.call-start = ((), (), s32[]{:S(2)}) async-start(), calls=%async_computation.3 | async-start | bytes 1638400 | tf_op jit(solution)/shard_map/all_gather | solution.py:134
  10.6 1.7 copy-start.4
  12.1 134.0 %all-gather.5.cloned.1.call-start = ((), (), s32[]{:S(2)}) async-start(), calls=%async_computation.4 | async-start | bytes 5308416 | tf_op jit(solution)/shard_map/all_gather | solution.py:197
  44.3 20.4 %copy-start.6 = (f32[1024]{0:T(1024)S(1)}, f32[1024]{0:T(1024)}, u32[]{:S(2)}) copy-start(f32[1024]{0:T(1024)} %param.29) | copy-start | bytes 12292
  50.8 5.3 %collective-permute-start = (bf16[64,128]{1,0:T(8,128)(2,1)S(1)}, bf16[64,128]{1,0:T(8,128)(2,1)S(1)}, u32[]{:S(2)}, u32[]{:S(2)}) collective-permute-start(bf16[64,128]{1,0:T(8,128)(2,1)S(1)} %copy.66), channel_id=1, source_target_pairs={{0,1},{1,0},{2,3},{3,2},{4,5},{5,4},{6,7},{7,6},{8,9},{9,8},{10,11... | collective-permute-start | bytes 49160 | tf_op jit(solution)/shard_map/ppermute | solution.py:87
  51.0 8.6 %collective-permute-start.1 = (bf16[64,128]{1,0:T(8,128)(2,1)S(1)}, bf16[64,128]{1,0:T(8,128)(2,1)S(1)}, u32[]{:S(2)}, u32[]{:S(2)}) collective-permute-start(bf16[64,128]{1,0:T(8,128)(2,1)S(1)} %copy.67), channel_id=1, source_target_pairs={{0,2},{1,3},{2,0},{3,1},{4,6},{5,7},{6,4},{7,5},{8,10},{9,11},{10,... | collective-permute-start | bytes 49160 | tf_op jit(solution)/shard_map/ppermute | solution.py:87
  52.6 7.3 %collective-permute-start.2 = (bf16[64,128]{1,0:T(8,128)(2,1)S(1)}, bf16[64,128]{1,0:T(8,128)(2,1)S(1)}, u32[]{:S(2)}, u32[]{:S(2)}) collective-permute-start(bf16[64,128]{1,0:T(8,128)(2,1)S(1)} %copy.68), channel_id=1, source_target_pairs={{0,3},{1,2},{2,1},{3,0},{4,7},{5,6},{6,5},{7,4},{8,11},{9,10},{10,... | collective-permute-start | bytes 49160 | tf_op jit(solution)/shard_map/ppermute | solution.py:87
  53.1 6.8 %collective-permute-start.3 = (bf16[64,128]{1,0:T(8,128)(2,1)S(1)}, bf16[64,128]{1,0:T(8,128)(2,1)S(1)}, u32[]{:S(2)}, u32[]{:S(2)}) collective-permute-start(bf16[64,128]{1,0:T(8,128)(2,1)S(1)} %copy.69), channel_id=1, source_target_pairs={{0,4},{1,5},{2,6},{3,7},{4,0},{5,1},{6,2},{7,3},{8,12},{9,13},{10,... | collective-permute-start | bytes 49160 | tf_op jit(solution)/shard_map/ppermute | solution.py:87
  55.7 4.3 %collective-permute-start.4 = (bf16[64,128]{1,0:T(8,128)(2,1)S(1)}, bf16[64,128]{1,0:T(8,128)(2,1)S(1)}, u32[]{:S(2)}, u32[]{:S(2)}) collective-permute-start(bf16[64,128]{1,0:T(8,128)(2,1)S(1)} %copy.70), channel_id=1, source_target_pairs={{0,5},{1,4},{2,7},{3,6},{4,1},{5,0},{6,3},{7,2},{8,13},{9,12},{10,... | collective-permute-start | bytes 49160 | tf_op jit(solution)/shard_map/ppermute | solution.py:87
  56.1 5.6 %collective-permute-start.5 = (bf16[64,128]{1,0:T(8,128)(2,1)S(1)}, bf16[64,128]{1,0:T(8,128)(2,1)S(1)}, u32[]{:S(2)}, u32[]{:S(2)}) collective-permute-start(bf16[64,128]{1,0:T(8,128)(2,1)S(1)} %copy.71), channel_id=1, source_target_pairs={{0,6},{1,7},{2,4},{3,5},{4,2},{5,3},{6,0},{7,1},{8,14},{9,15},{10,... | collective-permute-start | bytes 49160 | tf_op jit(solution)/shard_map/ppermute | solution.py:87
  59.5 5.0 %collective-permute-start.6 = (bf16[64,128]{1,0:T(8,128)(2,1)S(1)}, bf16[64,128]{1,0:T(8,128)(2,1)S(1)}, u32[]{:S(2)}, u32[]{:S(2)}) collective-permute-start(bf16[64,128]{1,0:T(8,128)(2,1)S(1)} %copy.72), channel_id=1, source_target_pairs={{0,7},{1,6},{2,5},{3,4},{4,3},{5,2},{6,1},{7,0},{8,15},{9,14},{10,... | collective-permute-start | bytes 49160 | tf_op jit(solution)/shard_map/ppermute | solution.py:87
  67.7 1.0 copy-start.1
  67.7 1.1 copy-start.5
  98.0 53.1 %copy-start.10 = (bf16[1,2048,256]{2,1,0:T(8,128)(2,1)S(1)}, bf16[1,2048,256]{2,1,0:T(8,128)(2,1)}, u32[]{:S(2)}) copy-start(bf16[1,2048,256]{2,1,0:T(8,128)(2,1)} %param.36) | copy-start | bytes 3145732
  98.1 116.6 %reduce-scatter.2.cloned.1.call-start = ((), (), s32[]{:S(2)}) async-start(), calls=%async_computation.5 | async-start | bytes 5308416 | tf_op jit(solution)/shard_map/reduce_scatter | solution.py:201
  160.9 59.8 %copy-start.7 = (f32[64,2]{0,1:T(2,128)S(1)}, f32[64,2]{0,1:T(2,128)}, u32[]{:S(2)}) copy-start(f32[64,2]{0,1:T(2,128)} %param.34) | copy-start | bytes 1540
  216.7 11.3 %all-to-all-start.1 = ((bf16[4,36,2048]{2,1,0:T(8,128)(2,1)}), bf16[4,36,2048]{2,1,0:T(8,128)(2,1)S(1)}, u32[]{:S(2)}, u32[]{:S(2)}) async-start(bf16[4,36,2048]{2,1,0:T(8,128)(2,1)} %reshape.245), calls=%async_computation.2 | async-start | bytes 1310720 | tf_op jit(solution)/shard_map/all_to_all | solution.py:207
Sparse Core Ops, SparseCore 0:
  12.3 31.2 all-gather.2
  98.2 47.8 all-gather.4
  161.0 53.6 reduce-scatter.1
